TPU v7x, 32 devices: a whole 2x2x4 slice. The times are simulated.
32 devices in a mesh: sp: 16 (over z, y, core), dp: 2 (over x).
Axes of the slice: x: 2, y: 2, z: 4, core: 2. Of those that a mesh axis runs over, the one named last changes fastest.
Arguments:
- signal: bfloat16 [2, 2048, 1024], P('dp', 'sp'), may hold values from -6 to 6
- pace: float32 [2, 16], P('dp'), may hold values from 0.5 to 2
- log_step: float32 [64], P('sp'), may hold values from -5.52 to -4.42
- a_real: float32 [64, 64], P('sp'), may hold values from -4 to -0.002, as said below
- a_imag: float32 [64, 64], P('sp'), may hold values from 0.5 to 201.06177
- in_map: float32 [64, 2, 64, 16], P('sp'), may hold values from -3 to 3
- out_map: float32 [64, 2, 16, 64], P('sp'), may hold values from -0.5 to 0.5
- skip: float32 [1024], P('sp'), may hold values from -1 to 1
- init_state: float32 [2, 2, 64, 64], P('dp', None, 'sp'), may hold values from -5 to 5
- w_glu: bfloat16 [1024, 1024], P('sp', 'dp'), may hold values from -0.1875 to 0.1875
- b_glu: float32 [1024], replicated, may hold values from -4 to 4
- g_mix: float32 [1024], replicated, may hold values from 0.1 to 1.9
- w_out: bfloat16 [1024, 4096], P('sp', 'dp'), may hold values from -0.1875 to 0.1875
Outputs:
- result: bfloat16 [2, 2048, 4096], P('dp', 'sp')
Inputs may be any that keep to these rules, and one draw needn't show every extreme that they name: `a_real`: negative entries; within a group all entries are of one order.
All inputs are finite; a program needn't handle non-finite values.
Results may differ from a plain program's by a relative error of at most 0.0075.
Values may be sent and summed in bfloat16 or wider, within the bound.
A program may use at most 64 MiB of HBM per device.

v0:
```python
import jax
import jax.numpy as jnp
from jax import lax
from jax.sharding import PartitionSpec as P


def combine(first, second):
    a1r, a1i, b1r, b1i = first
    a2r, a2i, b2r, b2i = second
    return (
        a2r * a1r - a2i * a1i,
        a2r * a1i + a2i * a1r,
        a2r * b1r - a2i * b1i + b2r,
        a2r * b1i + a2i * b1r + b2i,
    )


def mix_group(series, pace_row, log_rate, a_re, a_im, in_map, out_map, skip_row, init):
    blocks_count = pace_row.shape[0]
    length = series.shape[0]
    span = length // blocks_count
    states = a_re.shape[0]
    steps = (jnp.exp(log_rate) * pace_row)[:, None]
    decay = jnp.exp(a_re * steps)
    bar_re = decay * jnp.cos(a_im * steps)
    bar_im = decay * jnp.sin(a_im * steps)
    modulus = a_re * a_re + a_im * a_im
    coef_re = ((bar_re - 1.0) * a_re + bar_im * a_im) / modulus
    coef_im = (bar_im * a_re - (bar_re - 1.0) * a_im) / modulus
    drive_re = coef_re[..., None] * in_map[0] - coef_im[..., None] * in_map[1]
    drive_im = coef_re[..., None] * in_map[1] + coef_im[..., None] * in_map[0]
    drive = jnp.concatenate([drive_re, drive_im], axis=1).astype(jnp.bfloat16)
    blocks = series.reshape(blocks_count, span, series.shape[1])
    inject = jnp.einsum("kpc,ksc->kps", drive, blocks, preferred_element_type=jnp.float32)
    inner_re = inject[:, :states]
    inner_im = inject[:, states:]
    power_re = bar_re[..., None]
    power_im = bar_im[..., None]
    offset = 1
    while offset < span:
        moved_re = jnp.pad(inner_re[..., :-offset], ((0, 0), (0, 0), (offset, 0)))
        moved_im = jnp.pad(inner_im[..., :-offset], ((0, 0), (0, 0), (offset, 0)))
        inner_re, inner_im = (
            inner_re + power_re * moved_re - power_im * moved_im,
            inner_im + power_re * moved_im + power_im * moved_re,
        )
        power_re, power_im = (power_re * power_re - power_im * power_im, 2.0 * power_re * power_im)
        offset = offset * 2
    ends_re = (
        inner_re[:, :, -1].at[0].add(power_re[0, :, 0] * init[0] - power_im[0, :, 0] * init[1])
    )
    ends_im = (
        inner_im[:, :, -1].at[0].add(power_re[0, :, 0] * init[1] + power_im[0, :, 0] * init[0])
    )
    carried = lax.associative_scan(
        combine, (power_re[..., 0], power_im[..., 0], ends_re, ends_im), axis=0
    )
    before_re = jnp.concatenate([init[0][None], carried[2][:-1]], axis=0)[..., None]
    before_im = jnp.concatenate([init[1][None], carried[3][:-1]], axis=0)[..., None]
    places = (jnp.arange(span, dtype=jnp.float32) + 1.0)[None, None, :]
    scaled = steps[:, :, None] * places
    magnitude = jnp.exp(a_re[None, :, None] * scaled)
    angle = a_im[None, :, None] * scaled
    lift_re = magnitude * jnp.cos(angle)
    lift_im = magnitude * jnp.sin(angle)
    state_re = inner_re + lift_re * before_re - lift_im * before_im
    state_im = inner_im + lift_re * before_im + lift_im * before_re
    highest = lax.Precision.HIGHEST
    response = jnp.einsum("cp,kps->ksc", out_map[0], state_re, precision=highest) - jnp.einsum(
        "cp,kps->ksc", out_map[1], state_im, precision=highest
    )
    response = response.reshape(length, series.shape[1]) + skip_row * series.astype(jnp.float32)
    return jax.nn.gelu(response).astype(jnp.bfloat16)


def folder(left, piece):
    return jnp.dot(left, piece, preferred_element_type=jnp.float32)


def per_device(
    signal,
    pace,
    log_step,
    a_real,
    a_imag,
    in_map,
    out_map,
    skip,
    init_state,
    w_glu,
    b_glu,
    g_mix,
    w_out,
):
    local_seqs = signal.shape[0]
    tokens = signal.shape[1]
    width = signal.shape[2]
    groups = a_real.shape[0]
    channels = width // (groups * lax.axis_size("sp"))
    grouped = lax.all_to_all(signal, "sp", split_axis=2, concat_axis=1, tiled=True)
    length = grouped.shape[1]
    skips = skip.reshape(groups, channels)

    def per_sequence(inputs):
        sample, pace_row, init_row = inputs
        series = sample.reshape(length, groups, channels)
        outputs = jax.vmap(mix_group, in_axes=(1, None, 0, 0, 0, 0, 0, 0, 1), out_axes=1)(
            series, pace_row, log_step, a_real, a_imag, in_map, out_map, skips, init_row
        )
        return outputs.reshape(length, groups * channels)

    local_act = lax.map(per_sequence, (grouped, pace, init_state))
    activated = lax.all_to_all(local_act, "sp", split_axis=1, concat_axis=2, tiled=True)
    rows = activated.reshape(local_seqs * tokens, width)
    glu_cols, out_cols = (
        lax.all_gather(w_glu, "dp", axis=1, tiled=True),
        lax.all_gather(w_out, "dp", axis=1, tiled=True),
    )
    gate_pre = folder(rows, lax.all_gather(glu_cols, "sp", axis=0, tiled=True)) + b_glu
    gated = rows.astype(jnp.float32) * jax.nn.sigmoid(gate_pre)
    scale = lax.rsqrt(jnp.mean(gated * gated, axis=-1, keepdims=True) + 1e-06)
    mixed = (gated * scale * g_mix).astype(jnp.bfloat16)
    output = folder(mixed, lax.all_gather(out_cols, "sp", axis=0, tiled=True)).astype(jnp.bfloat16)
    return output.reshape(local_seqs, tokens, output.shape[1])


def solution(mesh):
    in_specs = (
        P("dp", "sp", None),
        P("dp", None),
        P("sp"),
        P("sp", None),
        P("sp", None),
        P("sp", None, None, None),
        P("sp", None, None, None),
        P("sp"),
        P("dp", None, "sp", None),
        P("sp", "dp"),
        P(),
        P(),
        P("sp", "dp"),
    )
    out_specs = P("dp", "sp", None)
    return jax.shard_map(
        per_device, mesh=mesh, in_specs=in_specs, out_specs=out_specs, check_vma=False
    )
```

profile of v0, /device:TPU:0, one launch (start us, length us, event | category | flops | bytes accessed | tf_op | source)
XLA Modules:
  0.0 147.8 jit_solution(5512769175658030008)
XLA Ops:
  6.5 0.0 all-gather.3.cloned.1.call-start
  6.5 7.8 %all_gather.12 = bf16[64,1024]{1,0:T(8,128)(2,1)} all-gather(bf16[64,512]{1,0:T(8,128)(2,1)} %param.26), channel_id=1, replica_groups=mesh['sp'=16,'dp'=2] {'dp'}, dimensions={1}, use_global_device_ids=true | all-gather | bytes 196608 | tf_op jit(solution)/shard_map/all_gather | solution.py:116
  14.3 0.0 all-gather.3.cloned.1.call-update
  14.3 0.0 all-gather.5.cloned.1.call-start
  14.4 8.4 %all_gather.14 = bf16[64,4096]{1,0:T(8,128)(2,1)} all-gather(bf16[64,2048]{1,0:T(8,128)(2,1)} %param.29), channel_id=1, replica_groups=mesh['sp'=16,'dp'=2] {'dp'}, dimensions={1}, use_global_device_ids=true | all-gather | bytes 786432 | tf_op jit(solution)/shard_map/all_gather | solution.py:117
  22.8 0.0 all-gather.5.cloned.1.call-update
  22.8 1.3 copy.90
  24.1 0.0 copy-start.5
  24.1 0.5 broadcast.764
  24.6 2.2 %reduce.14 = bf16[1024,128]{1,0:T(8,128)(2,1)S(1)} reduce(bf16[1024,1,128]{2,1,0:T(2,128)(2,1)S(1)} %bitcast.149, bf16[]{:T(256)} %broadcast.764), dimensions={1}, to_apply=%bitcast.92.reduce_sub_computation | reduce | bytes 524290
  26.8 0.8 reshape.452
  27.5 6.2 %all-to-all-start = ((bf16[16,2,4096]{2,1,0:T(2,128)(2,1)}), bf16[16,2,4096]{2,1,0:T(2,128)(2,1)S(1)}, u32[]{:S(2)}, u32[]{:S(2)}) async-start(bf16[16,2,4096]{2,1,0:T(2,128)(2,1)} %reshape.452), calls=%async_computation | async-start | bytes 524288 | tf_op jit(solution)/shard_map/all_to_all | solution.py:100
  33.7 0.0 copy-done.10
  33.8 0.0 copy-done.7
  33.8 0.1 broadcast_multiply_fusion.7
  33.8 0.1 copy.93
  33.9 0.0 copy-done.4
  33.9 0.1 multiply_exponential_fusion.1
  34.0 0.3 multiply_sine_fusion.2
  34.4 0.1 copy_multiply_fusion.10
  34.4 0.3 broadcast_multiply_fusion.4
  35.0 0.1 broadcast_multiply_fusion.6
  35.1 0.3 multiply_subtract_fusion.6
  35.5 0.1 mul.2235
  35.6 0.1 subtract_convert_fusion
  35.7 8.1 %all-to-all-done = bf16[16,2,4096]{2,1,0:T(2,128)(2,1)S(1)} async-done(((bf16[16,2,4096]{2,1,0:T(2,128)(2,1)}), bf16[16,2,4096]{2,1,0:T(2,128)(2,1)S(1)}, u32[]{:S(2)}, u32[]{:S(2)}) %all-to-all-start) | async-done | bytes 262176 | tf_op jit(solution)/shard_map/all_to_all | solution.py:100
  43.8 0.3 reshape.453
  44.1 0.2 copy.91
  44.3 0.1 reshape.439
  44.4 1.4 fusion.48
  45.9 0.6 fusion.80
  46.5 2.5 %fusion.4 = (f32[4,16,64,128]{3,2,1,0:T(8,128)S(1)}, f32[4,16,64,128]{3,2,1,0:T(8,128)S(1)}) fusion(f32[4,16,128,128]{3,2,1,0:T(8,128)S(1)} %fusion.48, f32[4,16,64,127]{3,2,1,0:T(8,128)S(1)} %get-tuple-element.102, f32[4,16,64,127]{3,2,1,0:T(8,128)S(1)} %get-tuple-element.101, f32[4,16,64]{2,1,0:T(8,128)S(1)} %get-tuple-element.151, ...), kind=kLoop, calls=%fused_computation.11 | loop fusion | flops 4194304 | bytes 12582912 | tf_op jit(solution)/shard_map/while/body/eval_jaxpr/vmap()/sub | solution.py:44
  49.0 2.5 %multiply_subtract_fusion.5 = (f32[4,16,64,128]{3,2,1,0:T(8,128)S(1)}, f32[4,16,64,128]{3,2,1,0:T(8,128)S(1)}) fusion(f32[4,16,64,128]{3,2,1,0:T(8,128)S(1)} %get-tuple-element.87, f32[4,16,64,126]{3,2,1,0:T(8,128)S(1)} %bitcast.135, f32[4,16,64,126]{3,2,1,0:T(8,128)S(1)} %bitcast.134, f32[4,16,64]{2,1,0:T(8,128)S(1)} %get-tuple-element.152, ...), kind=kLoop, calls=%fused_computation.34 | loop fusion | flops 4194304 | bytes 12550144 | tf_op jit(solution)/shard_map/while/body/eval_jaxpr/vmap()/sub | solution.py:44
  51.5 2.5 %multiply_subtract_fusion.4 = (f32[4,16,64,128]{3,2,1,0:T(8,128)S(1)}, f32[4,16,64,128]{3,2,1,0:T(8,128)S(1)}) fusion(f32[4,16,64,128]{3,2,1,0:T(8,128)S(1)} %get-tuple-element.99, f32[4,16,64,124]{3,2,1,0:T(8,128)S(1)} %bitcast.139, f32[4,16,64,124]{3,2,1,0:T(8,128)S(1)} %bitcast.138, f32[4,16,64]{2,1,0:T(8,128)S(1)} %get-tuple-element.148, ...), kind=kLoop, calls=%fused_computation.32 | loop fusion | flops 4194304 | bytes 12484608 | tf_op jit(solution)/shard_map/while/body/eval_jaxpr/vmap()/sub | solution.py:44
  54.1 2.5 %multiply_subtract_fusion.3 = (f32[4,16,64,128]{3,2,1,0:T(8,128)S(1)}, f32[4,16,64,128]{3,2,1,0:T(8,128)S(1)}) fusion(f32[4,16,64,128]{3,2,1,0:T(8,128)S(1)} %get-tuple-element.97, f32[4,16,64,120]{3,2,1,0:T(8,128)S(1)} %bitcast.141, f32[4,16,64,120]{3,2,1,0:T(8,128)S(1)} %bitcast.140, f32[4,16,64]{2,1,0:T(8,128)S(1)} %get-tuple-element.146, ...), kind=kLoop, calls=%fused_computation.30 | loop fusion | flops 4194304 | bytes 12353536 | tf_op jit(solution)/shard_map/while/body/eval_jaxpr/vmap()/sub | solution.py:44
  56.6 2.5 %multiply_subtract_fusion.2 = (f32[4,16,64,128]{3,2,1,0:T(8,128)S(1)}, f32[4,16,64,128]{3,2,1,0:T(8,128)S(1)}) fusion(f32[4,16,64,128]{3,2,1,0:T(8,128)S(1)} %get-tuple-element.95, f32[4,16,64,112]{3,2,1,0:T(8,128)S(1)} %bitcast.143, f32[4,16,64,112]{3,2,1,0:T(8,128)S(1)} %bitcast.142, f32[4,16,64]{2,1,0:T(8,128)S(1)} %get-tuple-element.144, ...), kind=kLoop, calls=%fused_computation.28 | loop fusion | flops 4194304 | bytes 12091392 | tf_op jit(solution)/shard_map/while/body/eval_jaxpr/vmap()/sub | solution.py:44
  59.1 2.5 %multiply_subtract_fusion.1 = (f32[4,16,64,128]{3,2,1,0:T(8,128)S(1)}, f32[4,16,64,128]{3,2,1,0:T(8,128)S(1)}) fusion(f32[4,16,64,128]{3,2,1,0:T(8,128)S(1)} %get-tuple-element.93, f32[4,16,64,96]{3,2,1,0:T(8,128)S(1)} %bitcast.145, f32[4,16,64,96]{3,2,1,0:T(8,128)S(1)} %bitcast.144, f32[4,16,64]{2,1,0:T(8,128)S(1)} %get-tuple-element.142, ...), kind=kLoop, calls=%fused_computation.26 | loop fusion | flops 4194304 | bytes 11567104 | tf_op jit(solution)/shard_map/while/body/eval_jaxpr/vmap()/sub | solution.py:44
  61.7 2.5 %multiply_subtract_fusion = (f32[4,16,64,128]{3,2,1,0:T(8,128)S(1)}, f32[4,16,64,128]{3,2,1,0:T(8,128)S(1)}) fusion(f32[4,16,64,128]{3,2,1,0:T(8,128)S(1)} %get-tuple-element.91, f32[4,16,64,64]{3,2,1,0:T(8,128)S(1)} %bitcast.137, f32[4,16,64,64]{3,2,1,0:T(8,128)S(1)} %bitcast.136, f32[4,16,64]{2,1,0:T(8,128)S(1)} %get-tuple-element.140, ...), kind=kLoop, calls=%fused_computation.24 | loop fusion | flops 4194304 | bytes 10518528 | tf_op jit(solution)/shard_map/while/body/eval_jaxpr/vmap()/sub | solution.py:44
  64.2 0.0 copy-start
  64.2 0.3 slice_reduce_fusion.2
  64.5 2.2 %slice_reduce_fusion = (f32[4,16,64]{2,1,0:T(8,128)S(1)}, f32[4,16,64]{2,1,0:T(8,128)S(1)}) fusion(f32[4,16,64,128]{3,2,1,0:T(8,128)S(1)} %get-tuple-element.90, f32[4,16,64,128]{3,2,1,0:T(8,128)S(1)} %get-tuple-element.89), kind=kLoop, calls=%fused_computation.6 | loop fusion | bytes 65536 | tf_op jit(solution)/shard_map/while/body/eval_jaxpr/vmap()/slice | solution.py:53
  66.7 0.0 copy-start.8
  66.8 0.3 scatter-add.6
  67.8 0.1 pad.155
  67.9 0.1 pad.156
  67.9 0.1 pad.154
  68.0 0.1 pad.153
  68.6 11.0 %fusion.5 = f32[4,16,128,16]{2,3,1,0:T(8,128)S(1)} fusion(f32[4,16,64,128]{3,2,1,0:T(8,128)} %copy-done, f32[4,16,64]{2,1,0:T(8,128)S(1)} %pad_maximum_fusion.1, f32[4,16,64]{2,1,0:T(8,128)S(1)} %pad_maximum_fusion, f32[4,64]{1,0:T(4,128)S(1)} %copy-done.3, f32[4,16,128]{2,1,0:T(8,128)S(1)} %broadcast_multiply_fusion.6, f32[4,64]{1,0:T(4,128)S(1)} %copy-done.4, ...), kind=kOutput, calls=%fused_computation.12 | convolution fusion | flops 104857600 | bytes 2756608 | tf_op jit(solution)/shard_map/while/body/eval_jaxpr/vmap(cp,kps->ksc)/dot_general | solution.py:69
  79.6 9.9 %fusion.22 = f32[4,16,2,8,128]{4,3,2,1,0:T(8,128)S(1)} fusion(f32[4,16,128,16]{2,3,1,0:T(8,128)S(1)} %fusion.5, f32[4,16,64,128]{3,2,1,0:T(8,128)S(1)} %get-tuple-element.89, f32[4,16,64]{2,1,0:T(8,128)S(1)} %pad_maximum_fusion.1, f32[4,16,64]{2,1,0:T(8,128)S(1)} %pad_maximum_fusion, f32[4,64]{1,0:T(4,128)S(1)} %copy-done.3, ...), kind=kOutput, calls=%fused_computation.36 | convolution fusion | flops 104988672 | bytes 3280896 | tf_op jit(solution)/shard_map/while/body/eval_jaxpr/vmap(cp,kps->ksc)/dot_general | solution.py:69
  89.6 0.3 fusion.47
  89.9 0.7 copy.127
  90.6 11.4 %reduce.15 = bf16[2048,64]{1,0:T(8,128)(2,1)S(1)} reduce(bf16[2048,1,64]{2,1,0:T(2,128)(2,1)S(1)} %bitcast.147, bf16[]{:T(256)} %broadcast.764), dimensions={1}, to_apply=%bitcast.94.reduce_sub_computation | reduce | bytes 524290
  102.1 0.4 reshape.454
  102.5 20.1 %all_to_all.30 = bf16[16,2,4096]{2,1,0:T(2,128)(2,1)S(1)} all-to-all(bf16[16,2,4096]{2,1,0:T(2,128)(2,1)S(1)} %reshape.454), channel_id=1, replica_groups=mesh['sp'=16,'dp'=2] {'sp'}, dimensions={0} | all-to-all | bytes 524288 | tf_op jit(solution)/shard_map/all_to_all | solution.py:113
  122.6 0.6 reshape.455
  123.2 0.6 copy.128
  123.9 0.1 copy.129
  124.0 0.1 copy.130
  124.1 0.0 copy-start.1
  124.1 0.0 all-gather.3.cloned.1.call-done
  124.2 2.2 %multiply_reduce_fusion = (f32[128]{0:T(128)S(1)}, f32[128,1024]{1,0:T(8,128)S(1)}) fusion(f32[1024]{0:T(1024)S(1)} %copy-done.9, bf16[128,1024]{0,1:T(8,128)(2,1)S(1)} %bitcast.153, bf16[1024,1024]{1,0:T(8,128)(2,1)} %all-gather.3.cloned.1.call-done, bf16[128,1024]{1,0:T(8,128)(2,1)S(1)} %copy.130), kind=kOutput, calls=%fused_computation.64 | convolution fusion | flops 269483904 | bytes 3150336 | tf_op jit(solution)/shard_map/dot_general | solution.py:77
  126.4 8.8 %all-gather.5.cloned.1.call-done = bf16[1024,4096]{1,0:T(8,128)(2,1)} async-done(((bf16[64,4096]{1,0:T(8,128)(2,1)}), bf16[1024,4096]{1,0:T(8,128)(2,1)}) %all-gather.5.cloned.1.call-update) | async-done | bytes 8388624 | tf_op jit(solution)/shard_map/all_gather | solution.py:123
  135.3 0.0 copy-done.1
  135.3 5.7 %fusion = bf16[1,128,4096]{2,1,0:T(8,128)(2,1)} fusion(bf16[1024,4096]{1,0:T(8,128)(2,1)} %all-gather.5.cloned.1.call-done, f32[128,1024]{1,0:T(8,128)S(1)} %get-tuple-element.161, f32[1024]{0:T(1024)S(1)} %copy-done.1, f32[128]{0:T(128)S(1)} %add_rsqrt_fusion), kind=kOutput, calls=%fused_computation.1 | convolution fusion | flops 1074659328 | bytes 9966080 | tf_op jit(solution)/shard_map/dot_general | solution.py:77
  (100 shorter events, 1.6 us)
Async XLA Ops:
  6.5 27.2 %copy-start.10 = (f32[4]{0:T(128)S(1)}, f32[4]{0:T(128)}, u32[]{:S(2)}) copy-start(f32[4]{0:T(128)} %param.19) | copy-start | bytes 52
  6.5 27.2 %copy-start.7 = (f32[1,16]{1,0:T(1,128)S(1)}, f32[1,16]{1,0:T(1,128)}, u32[]{:S(2)}) copy-start(f32[1,16]{1,0:T(1,128)} %param.18) | copy-start | bytes 196
  6.5 27.4 %copy-start.4 = (f32[4,64]{1,0:T(4,128)S(1)}, f32[4,64]{1,0:T(4,128)}, u32[]{:S(2)}) copy-start(f32[4,64]{1,0:T(4,128)} %param.20) | copy-start | bytes 3076
  6.5 117.6 %all-gather.3.cloned.1.call-start = ((), (), s32[]{:S(2)}) async-start(), calls=%async_computation.2 | async-start | bytes 2228224 | tf_op jit(solution)/shard_map/all_gather | solution.py:119
  14.3 19.7 %copy-start.3 = (f32[4,64]{1,0:T(4,128)S(1)}, f32[4,64]{1,0:T(4,128)}, u32[]{:S(2)}) copy-start(f32[4,64]{1,0:T(4,128)} %param.21) | copy-start | bytes 3076
  14.3 120.9 %all-gather.5.cloned.1.call-start = ((), (), s32[]{:S(2)}) async-start(), calls=%async_computation.3 | async-start | bytes 8912896 | tf_op jit(solution)/shard_map/all_gather | solution.py:123
  24.1 11.3 %copy-start.5 = (f32[1,2,4,64]{3,2,1,0:T(4,128)S(1)}, f32[1,2,4,64]{3,2,1,0:T(4,128)}, u32[]{:S(2)}) copy-start(f32[1,2,4,64]{3,2,1,0:T(4,128)} %param.25) | copy-start | bytes 6148
  24.6 10.9 %copy-start.6 = (f32[64]{0:T(128)S(1)}, f32[64]{0:T(128)}, u32[]{:S(2)}) copy-start(f32[64]{0:T(128)} %param.24) | copy-start | bytes 772
  24.6 11.0 %copy-start.2 = (f32[4,2,64,16]{2,3,1,0:T(8,128)S(1)}, f32[4,2,64,16]{2,3,1,0:T(8,128)}, u32[]{:S(2)}) copy-start(f32[4,2,64,16]{2,3,1,0:T(8,128)} %param.22) | copy-start | bytes 98308
  27.5 16.3 %all-to-all-start = ((bf16[16,2,4096]{2,1,0:T(2,128)(2,1)}), bf16[16,2,4096]{2,1,0:T(2,128)(2,1)S(1)}, u32[]{:S(2)}, u32[]{:S(2)}) async-start(bf16[16,2,4096]{2,1,0:T(2,128)(2,1)} %reshape.452), calls=%async_computation | async-start | bytes 524288 | tf_op jit(solution)/shard_map/all_to_all | solution.py:100
  64.2 2.6 %copy-start = (f32[4,16,64,128]{3,2,1,0:T(8,128)}, f32[4,16,64,128]{3,2,1,0:T(8,128)S(1)}, u32[]{:S(2)}) copy-start(f32[4,16,64,128]{3,2,1,0:T(8,128)S(1)} %get-tuple-element.90) | copy-start | bytes 6291460
  66.7 1.8 %copy-start.8 = (f32[4,2,16,64]{3,2,1,0:T(8,128)S(1)}, f32[4,2,16,64]{3,2,1,0:T(8,128)}, u32[]{:S(2)}) copy-start(f32[4,2,16,64]{3,2,1,0:T(8,128)} %param.23) | copy-start | bytes 98308
  122.6 1.6 %copy-start.9 = (f32[1024]{0:T(1024)S(1)}, f32[1024]{0:T(1024)}, u32[]{:S(2)}) copy-start(f32[1024]{0:T(1024)} %param.27) | copy-start | bytes 12292
  124.1 11.2 %copy-start.1 = (f32[1024]{0:T(1024)S(1)}, f32[1024]{0:T(1024)}, u32[]{:S(2)}) copy-start(f32[1024]{0:T(1024)} %param.28) | copy-start | bytes 12292
Sparse Core Ops, SparseCore 0:
  14.5 41.9 all-gather.2
  58.6 76.6 all-gather.4
where the time goes:
time: 148 us
  blocking collectives  36.3 us (25%)
  other arithmetic  33.4 us (23%)
  matrix products  30.3 us (20%)
  waiting for transfers between devices  17 us (11%)
  between operations  14.1 us (10%)
  local copies, waits for them, and re-layouts  10.5 us (7%)
  starting transfers between devices  6.23 us (4%)
    all_to_all x1, blocking collectives, per_device(): lax.all_to_all(local_act, 'sp', split_axis=1, concat_axis=2, tiled=True)  20.1 us
    sub x7, other arithmetic, mix_group(): inner_re + power_re * moved_re - power_im * moved_im  17.7 us
    unnamed x2, other arithmetic  13.6 us
    dot_general x1, matrix products, mix_group(): jnp.einsum('cp,kps->ksc', out_map[1], state_im, precision=highest)  11 us
    dot_general x1, matrix products, mix_group(): jnp.einsum('cp,kps->ksc', out_map[0], state_re, precision=highest)  9.95 us
    all_gather x1, waiting for transfers between devices, per_device(): lax.all_gather(out_cols, 'sp', axis=0, tiled=True)  8.84 us
    all_gather x1, blocking collectives, per_device(): lax.all_gather(w_out, 'dp', axis=1, tiled=True)  8.38 us
    all_to_all x1, waiting for transfers between devices, per_device(): lax.all_to_all(signal, 'sp', split_axis=2, concat_axis=1, tiled=True)  8.07 us
  transfers between devices with their start and end apart: 3, of which 2 were waited for; matrix products, arithmetic and copies ran while one was open for 46% of the time, Pallas kernels for 0%

commit v1 on v0

--- a/solution.py
+++ b/solution.py
@@ -113,7 +113,7 @@
     activated = lax.all_to_all(local_act, "sp", split_axis=1, concat_axis=2, tiled=True)
     rows = activated.reshape(local_seqs * tokens, width)
     glu_cols, out_cols = (
-        lax.all_gather(w_glu, "dp", axis=1, tiled=True),
+        jnp.concatenate(lax.all_gather(w_glu, "dp"), axis=1),
         lax.all_gather(w_out, "dp", axis=1, tiled=True),
     )
     gate_pre = folder(rows, lax.all_gather(glu_cols, "sp", axis=0, tiled=True)) + b_glu

time: 148 us -> 149 us (level)
  waiting for transfers between devices: 17 us -> 20.3 us
  blocking collectives: 36.3 us -> 33.6 us
    all_gather x1, waiting for transfers between devices: 8.84 us -> 12.1 us  [per_device(): lax.all_gather(out_cols, 'sp', axis=0, tiled=True)]
    all_to_all x1, blocking collectives: 20.1 us -> 17.5 us  [per_device(): lax.all_to_all(local_act, 'sp', split_axis=1, concat_axis=2, tiled=True)]
    all_gather x1, blocking collectives: 7.76 us -> 6.26 us  [per_device(): lax.all_gather(w_glu, 'dp')]
    unnamed x32 -> x35, local copies, waits for them, and re-layouts: 3.99 us -> 3.85 us
where the time goes in v1:
time: 149 us; the launch traced here: 148 us
  blocking collectives  33.6 us (23%)
  other arithmetic  33.5 us (22%)
  matrix products  30.4 us (20%)
  waiting for transfers between devices  20.3 us (14%)
  between operations  14.1 us (9%)
  local copies, waits for them, and re-layouts  10.5 us (7%)
  starting transfers between devices  5.99 us (4%)
    all_to_all x1, blocking collectives, per_device(): lax.all_to_all(local_act, 'sp', split_axis=1, concat_axis=2, tiled=True)  17.5 us
    sub x7, other arithmetic, mix_group(): inner_re + power_re * moved_re - power_im * moved_im  17.5 us
    unnamed x2, other arithmetic  13.8 us
    all_gather x1, waiting for transfers between devices, per_device(): lax.all_gather(out_cols, 'sp', axis=0, tiled=True)  12.1 us
    dot_general x1, matrix products, mix_group(): jnp.einsum('cp,kps->ksc', out_map[1], state_im, precision=highest)  11 us
    dot_general x1, matrix products, mix_group(): jnp.einsum('cp,kps->ksc', out_map[0], state_re, precision=highest)  9.95 us
    all_gather x1, blocking collectives, per_device(): lax.all_gather(w_out, 'dp', axis=1, tiled=True)  9.76 us
    all_to_all x1, waiting for transfers between devices, per_device(): lax.all_to_all(signal, 'sp', split_axis=2, concat_axis=1, tiled=True)  8.07 us
  transfers between devices with their start and end apart: 3, of which 2 were waited for; matrix products, arithmetic and copies ran while one was open for 46% of the time, Pallas kernels for 0%

profile of v1, /device:TPU:0, one launch (start us, length us, event | category | flops | bytes accessed | tf_op | source)
XLA Modules:
  0.0 148.2 jit_solution(15398461946471370925)
XLA Ops:
  6.5 6.3 %all-gather = bf16[128,512]{1,0:T(8,128)(2,1)S(1)} all-gather(bf16[64,512]{1,0:T(8,128)(2,1)} %param.26), channel_id=2, replica_groups=mesh['sp'=16,'dp'=2] {'dp'}, dimensions={0}, use_global_device_ids=true | all-gather | bytes 196608 | tf_op jit(solution)/shard_map/all_gather | solution.py:116
  12.8 0.1 copy.135
  12.9 0.7 copy.147
  13.6 0.0 all-gather.4.cloned.1.call-update
  13.6 0.0 all-gather.6.cloned.1.call-start
  13.7 9.8 %all_gather.18 = bf16[64,4096]{1,0:T(8,128)(2,1)} all-gather(bf16[64,2048]{1,0:T(8,128)(2,1)} %param.29), channel_id=1, replica_groups=mesh['sp'=16,'dp'=2] {'dp'}, dimensions={1}, use_global_device_ids=true | all-gather | bytes 786432 | tf_op jit(solution)/shard_map/all_gather | solution.py:117
  23.5 0.0 all-gather.6.cloned.1.call-update
  23.5 0.4 copy.94
  23.9 0.0 copy-start.6
  23.9 0.5 broadcast.764
  24.4 2.3 %reduce.14 = bf16[1024,128]{1,0:T(8,128)(2,1)S(1)} reduce(bf16[1024,1,128]{2,1,0:T(2,128)(2,1)S(1)} %bitcast.153, bf16[]{:T(256)} %broadcast.764), dimensions={1}, to_apply=%bitcast.96.reduce_sub_computation | reduce | bytes 524290
  26.7 0.8 reshape.461
  27.5 5.9 %all-to-all-start = ((bf16[16,2,4096]{2,1,0:T(2,128)(2,1)}), bf16[16,2,4096]{2,1,0:T(2,128)(2,1)S(1)}, u32[]{:S(2)}, u32[]{:S(2)}) async-start(bf16[16,2,4096]{2,1,0:T(2,128)(2,1)} %reshape.461), calls=%async_computation | async-start | bytes 524288 | tf_op jit(solution)/shard_map/all_to_all | solution.py:100
  33.5 0.1 broadcast_multiply_fusion.7
  33.6 0.1 copy.97
  33.6 0.0 copy-done.5
  33.7 0.1 multiply_exponential_fusion.1
  33.7 0.3 multiply_sine_fusion.2
  34.1 0.1 copy_multiply_fusion.10
  34.2 0.3 broadcast_multiply_fusion.4
  34.8 0.1 broadcast_multiply_fusion.6
  34.8 0.3 multiply_subtract_fusion.6
  35.2 0.1 mul.2235
  35.3 0.0 copy-done.3
  35.3 0.1 subtract_convert_fusion
  35.5 8.1 %all-to-all-done = bf16[16,2,4096]{2,1,0:T(2,128)(2,1)S(1)} async-done(((bf16[16,2,4096]{2,1,0:T(2,128)(2,1)}), bf16[16,2,4096]{2,1,0:T(2,128)(2,1)S(1)}, u32[]{:S(2)}, u32[]{:S(2)}) %all-to-all-start) | async-done | bytes 262176 | tf_op jit(solution)/shard_map/all_to_all | solution.py:100
  43.5 0.3 reshape.462
  43.9 0.2 copy.95
  44.0 0.1 reshape.445
  44.2 1.4 fusion.48
  45.6 0.6 fusion.80
  46.2 2.5 %fusion.4 = (f32[4,16,64,128]{3,2,1,0:T(8,128)S(1)}, f32[4,16,64,128]{3,2,1,0:T(8,128)S(1)}) fusion(f32[4,16,128,128]{3,2,1,0:T(8,128)S(1)} %fusion.48, f32[4,16,64,127]{3,2,1,0:T(8,128)S(1)} %get-tuple-element.102, f32[4,16,64,127]{3,2,1,0:T(8,128)S(1)} %get-tuple-element.101, f32[4,16,64]{2,1,0:T(8,128)S(1)} %get-tuple-element.151, ...), kind=kLoop, calls=%fused_computation.11 | loop fusion | flops 4194304 | bytes 12582912 | tf_op jit(solution)/shard_map/while/body/eval_jaxpr/vmap()/sub | solution.py:44
  48.7 2.5 %multiply_subtract_fusion.5 = (f32[4,16,64,128]{3,2,1,0:T(8,128)S(1)}, f32[4,16,64,128]{3,2,1,0:T(8,128)S(1)}) fusion(f32[4,16,64,128]{3,2,1,0:T(8,128)S(1)} %get-tuple-element.87, f32[4,16,64,126]{3,2,1,0:T(8,128)S(1)} %bitcast.139, f32[4,16,64,126]{3,2,1,0:T(8,128)S(1)} %bitcast.138, f32[4,16,64]{2,1,0:T(8,128)S(1)} %get-tuple-element.152, ...), kind=kLoop, calls=%fused_computation.34 | loop fusion | flops 4194304 | bytes 12550144 | tf_op jit(solution)/shard_map/while/body/eval_jaxpr/vmap()/sub | solution.py:44
  51.2 2.5 %multiply_subtract_fusion.4 = (f32[4,16,64,128]{3,2,1,0:T(8,128)S(1)}, f32[4,16,64,128]{3,2,1,0:T(8,128)S(1)}) fusion(f32[4,16,64,128]{3,2,1,0:T(8,128)S(1)} %get-tuple-element.99, f32[4,16,64,124]{3,2,1,0:T(8,128)S(1)} %bitcast.143, f32[4,16,64,124]{3,2,1,0:T(8,128)S(1)} %bitcast.142, f32[4,16,64]{2,1,0:T(8,128)S(1)} %get-tuple-element.148, ...), kind=kLoop, calls=%fused_computation.32 | loop fusion | flops 4194304 | bytes 12484608 | tf_op jit(solution)/shard_map/while/body/eval_jaxpr/vmap()/sub | solution.py:44
  53.7 2.5 %multiply_subtract_fusion.3 = (f32[4,16,64,128]{3,2,1,0:T(8,128)S(1)}, f32[4,16,64,128]{3,2,1,0:T(8,128)S(1)}) fusion(f32[4,16,64,128]{3,2,1,0:T(8,128)S(1)} %get-tuple-element.97, f32[4,16,64,120]{3,2,1,0:T(8,128)S(1)} %bitcast.145, f32[4,16,64,120]{3,2,1,0:T(8,128)S(1)} %bitcast.144, f32[4,16,64]{2,1,0:T(8,128)S(1)} %get-tuple-element.146, ...), kind=kLoop, calls=%fused_computation.30 | loop fusion | flops 4194304 | bytes 12353536 | tf_op jit(solution)/shard_map/while/body/eval_jaxpr/vmap()/sub | solution.py:44
  56.2 2.5 %multiply_subtract_fusion.2 = (f32[4,16,64,128]{3,2,1,0:T(8,128)S(1)}, f32[4,16,64,128]{3,2,1,0:T(8,128)S(1)}) fusion(f32[4,16,64,128]{3,2,1,0:T(8,128)S(1)} %get-tuple-element.95, f32[4,16,64,112]{3,2,1,0:T(8,128)S(1)} %bitcast.147, f32[4,16,64,112]{3,2,1,0:T(8,128)S(1)} %bitcast.146, f32[4,16,64]{2,1,0:T(8,128)S(1)} %get-tuple-element.144, ...), kind=kLoop, calls=%fused_computation.28 | loop fusion | flops 4194304 | bytes 12091392 | tf_op jit(solution)/shard_map/while/body/eval_jaxpr/vmap()/sub | solution.py:44
  58.7 2.5 %multiply_subtract_fusion.1 = (f32[4,16,64,128]{3,2,1,0:T(8,128)S(1)}, f32[4,16,64,128]{3,2,1,0:T(8,128)S(1)}) fusion(f32[4,16,64,128]{3,2,1,0:T(8,128)S(1)} %get-tuple-element.93, f32[4,16,64,96]{3,2,1,0:T(8,128)S(1)} %bitcast.149, f32[4,16,64,96]{3,2,1,0:T(8,128)S(1)} %bitcast.148, f32[4,16,64]{2,1,0:T(8,128)S(1)} %get-tuple-element.142, ...), kind=kLoop, calls=%fused_computation.26 | loop fusion | flops 4194304 | bytes 11567104 | tf_op jit(solution)/shard_map/while/body/eval_jaxpr/vmap()/sub | solution.py:44
  61.2 2.5 %multiply_subtract_fusion = (f32[4,16,64,128]{3,2,1,0:T(8,128)S(1)}, f32[4,16,64,128]{3,2,1,0:T(8,128)S(1)}) fusion(f32[4,16,64,128]{3,2,1,0:T(8,128)S(1)} %get-tuple-element.91, f32[4,16,64,64]{3,2,1,0:T(8,128)S(1)} %bitcast.141, f32[4,16,64,64]{3,2,1,0:T(8,128)S(1)} %bitcast.140, f32[4,16,64]{2,1,0:T(8,128)S(1)} %get-tuple-element.140, ...), kind=kLoop, calls=%fused_computation.24 | loop fusion | flops 4194304 | bytes 10518528 | tf_op jit(solution)/shard_map/while/body/eval_jaxpr/vmap()/sub | solution.py:44
  63.8 0.3 slice_reduce_fusion.2
  64.1 2.2 %slice_reduce_fusion = (f32[4,16,64]{2,1,0:T(8,128)S(1)}, f32[4,16,64]{2,1,0:T(8,128)S(1)}) fusion(f32[4,16,64,128]{3,2,1,0:T(8,128)S(1)} %get-tuple-element.90, f32[4,16,64,128]{3,2,1,0:T(8,128)S(1)} %get-tuple-element.89), kind=kLoop, calls=%fused_computation.6 | loop fusion | bytes 65536 | tf_op jit(solution)/shard_map/while/body/eval_jaxpr/vmap()/slice | solution.py:53
  66.3 0.0 copy-done
  66.3 0.0 copy-start.9
  66.4 0.3 scatter-add.6
  67.4 0.1 pad.155
  67.4 0.1 pad.156
  67.5 0.1 pad.154
  67.6 0.1 pad.153
  68.2 11.0 %fusion.5 = f32[4,16,128,16]{2,3,1,0:T(8,128)S(1)} fusion(f32[4,16,64,128]{3,2,1,0:T(8,128)} %copy-done, f32[4,16,64]{2,1,0:T(8,128)S(1)} %pad_maximum_fusion.1, f32[4,16,64]{2,1,0:T(8,128)S(1)} %pad_maximum_fusion, f32[4,64]{1,0:T(4,128)S(1)} %copy-done.4, f32[4,16,128]{2,1,0:T(8,128)S(1)} %broadcast_multiply_fusion.6, f32[4,64]{1,0:T(4,128)S(1)} %copy-done.5, ...), kind=kOutput, calls=%fused_computation.12 | convolution fusion | flops 104857600 | bytes 2756608 | tf_op jit(solution)/shard_map/while/body/eval_jaxpr/vmap(cp,kps->ksc)/dot_general | solution.py:69
  79.2 10.0 %fusion.22 = f32[4,16,2,8,128]{4,3,2,1,0:T(8,128)S(1)} fusion(f32[4,16,128,16]{2,3,1,0:T(8,128)S(1)} %fusion.5, f32[4,16,64,128]{3,2,1,0:T(8,128)S(1)} %get-tuple-element.89, f32[4,16,64]{2,1,0:T(8,128)S(1)} %pad_maximum_fusion.1, f32[4,16,64]{2,1,0:T(8,128)S(1)} %pad_maximum_fusion, f32[4,64]{1,0:T(4,128)S(1)} %copy-done.4, ...), kind=kOutput, calls=%fused_computation.36 | convolution fusion | flops 104988672 | bytes 3280896 | tf_op jit(solution)/shard_map/while/body/eval_jaxpr/vmap(cp,kps->ksc)/dot_general | solution.py:69
  89.2 0.3 fusion.47
  89.5 0.7 copy.131
  90.2 11.5 %reduce.15 = bf16[2048,64]{1,0:T(8,128)(2,1)S(1)} reduce(bf16[2048,1,64]{2,1,0:T(2,128)(2,1)S(1)} %bitcast.151, bf16[]{:T(256)} %broadcast.764), dimensions={1}, to_apply=%bitcast.98.reduce_sub_computation | reduce | bytes 524290
  101.8 0.4 reshape.463
  102.2 17.5 %all_to_all.30 = bf16[16,2,4096]{2,1,0:T(2,128)(2,1)S(1)} all-to-all(bf16[16,2,4096]{2,1,0:T(2,128)(2,1)S(1)} %reshape.463), channel_id=1, replica_groups=mesh['sp'=16,'dp'=2] {'sp'}, dimensions={0} | all-to-all | bytes 524288 | tf_op jit(solution)/shard_map/all_to_all | solution.py:113
  119.7 0.6 reshape.464
  120.3 0.6 copy.132
  121.0 0.1 copy.133
  121.1 0.1 copy.134
  121.2 0.0 copy-start.2
  121.2 0.0 all-gather.4.cloned.1.call-done
  121.3 0.0 copy-done.10
  121.3 2.3 %multiply_reduce_fusion = (f32[128]{0:T(128)S(1)}, f32[128,1024]{1,0:T(8,128)S(1)}) fusion(f32[1024]{0:T(1024)S(1)} %copy-done.10, bf16[128,1024]{0,1:T(8,128)(2,1)S(1)} %bitcast.157, bf16[1024,1024]{1,0:T(8,128)(2,1)} %all-gather.4.cloned.1.call-done, bf16[128,1024]{1,0:T(8,128)(2,1)S(1)} %copy.134), kind=kOutput, calls=%fused_computation.64 | convolution fusion | flops 269483904 | bytes 3150336 | tf_op jit(solution)/shard_map/dot_general | solution.py:77
  123.6 12.1 %all-gather.6.cloned.1.call-done = bf16[1024,4096]{1,0:T(8,128)(2,1)} async-done(((bf16[64,4096]{1,0:T(8,128)(2,1)}), bf16[1024,4096]{1,0:T(8,128)(2,1)}) %all-gather.6.cloned.1.call-update) | async-done | bytes 8388624 | tf_op jit(solution)/shard_map/all_gather | solution.py:123
  135.7 5.7 %fusion = bf16[1,128,4096]{2,1,0:T(8,128)(2,1)} fusion(bf16[1024,4096]{1,0:T(8,128)(2,1)} %all-gather.6.cloned.1.call-done, f32[128,1024]{1,0:T(8,128)S(1)} %get-tuple-element.161, f32[1024]{0:T(1024)S(1)} %copy-done.2, f32[128]{0:T(128)S(1)} %add_rsqrt_fusion), kind=kOutput, calls=%fused_computation.1 | convolution fusion | flops 1074659328 | bytes 9966080 | tf_op jit(solution)/shard_map/dot_general | solution.py:77
  (104 shorter events, 1.6 us)
Async XLA Ops:
  6.5 16.9 %copy-start.1 = (bf16[1,128,1024]{2,1,0:T(8,128)(2,1)S(1)}, bf16[1,128,1024]{2,1,0:T(8,128)(2,1)}, u32[]{:S(2)}) copy-start(bf16[1,128,1024]{2,1,0:T(8,128)(2,1)} %param.17) | copy-start | bytes 786436
  6.5 114.7 %all-gather.4.cloned.1.call-start = ((), (), s32[]{:S(2)}) async-start(), calls=%async_computation.2 | async-start | bytes 2228224 | tf_op jit(solution)/shard_map/all_gather | solution.py:119
  13.6 19.9 %copy-start.11 = (f32[4]{0:T(128)S(1)}, f32[4]{0:T(128)}, u32[]{:S(2)}) copy-start(f32[4]{0:T(128)} %param.19) | copy-start | bytes 52
  13.6 19.9 %copy-start.8 = (f32[1,16]{1,0:T(1,128)S(1)}, f32[1,16]{1,0:T(1,128)}, u32[]{:S(2)}) copy-start(f32[1,16]{1,0:T(1,128)} %param.18) | copy-start | bytes 196
  13.6 20.0 %copy-start.5 = (f32[4,64]{1,0:T(4,128)S(1)}, f32[4,64]{1,0:T(4,128)}, u32[]{:S(2)}) copy-start(f32[4,64]{1,0:T(4,128)} %param.20) | copy-start | bytes 3076
  13.6 20.1 %copy-start.4 = (f32[4,64]{1,0:T(4,128)S(1)}, f32[4,64]{1,0:T(4,128)}, u32[]{:S(2)}) copy-start(f32[4,64]{1,0:T(4,128)} %param.21) | copy-start | bytes 3076
  13.6 122.1 %all-gather.6.cloned.1.call-start = ((), (), s32[]{:S(2)}) async-start(), calls=%async_computation.3 | async-start | bytes 8912896 | tf_op jit(solution)/shard_map/all_gather | solution.py:123
  23.9 11.2 %copy-start.6 = (f32[1,2,4,64]{3,2,1,0:T(4,128)S(1)}, f32[1,2,4,64]{3,2,1,0:T(4,128)}, u32[]{:S(2)}) copy-start(f32[1,2,4,64]{3,2,1,0:T(4,128)} %param.25) | copy-start | bytes 6148
  24.4 10.8 %copy-start.7 = (f32[64]{0:T(128)S(1)}, f32[64]{0:T(128)}, u32[]{:S(2)}) copy-start(f32[64]{0:T(128)} %param.24) | copy-start | bytes 772
  24.4 10.9 %copy-start.3 = (f32[4,2,64,16]{2,3,1,0:T(8,128)S(1)}, f32[4,2,64,16]{2,3,1,0:T(8,128)}, u32[]{:S(2)}) copy-start(f32[4,2,64,16]{2,3,1,0:T(8,128)} %param.22) | copy-start | bytes 98308
  27.5 16.0 %all-to-all-start = ((bf16[16,2,4096]{2,1,0:T(2,128)(2,1)}), bf16[16,2,4096]{2,1,0:T(2,128)(2,1)S(1)}, u32[]{:S(2)}, u32[]{:S(2)}) async-start(bf16[16,2,4096]{2,1,0:T(2,128)(2,1)} %reshape.461), calls=%async_computation | async-start | bytes 524288 | tf_op jit(solution)/shard_map/all_to_all | solution.py:100
  63.8 2.6 %copy-start = (f32[4,16,64,128]{3,2,1,0:T(8,128)}, f32[4,16,64,128]{3,2,1,0:T(8,128)S(1)}, u32[]{:S(2)}) copy-start(f32[4,16,64,128]{3,2,1,0:T(8,128)S(1)} %get-tuple-element.90) | copy-start | bytes 6291460
  66.3 1.8 %copy-start.9 = (f32[4,2,16,64]{3,2,1,0:T(8,128)S(1)}, f32[4,2,16,64]{3,2,1,0:T(8,128)}, u32[]{:S(2)}) copy-start(f32[4,2,16,64]{3,2,1,0:T(8,128)} %param.23) | copy-start | bytes 98308
  119.7 1.6 %copy-start.10 = (f32[1024]{0:T(1024)S(1)}, f32[1024]{0:T(1024)}, u32[]{:S(2)}) copy-start(f32[1024]{0:T(1024)} %param.27) | copy-start | bytes 12292
  121.2 14.5 %copy-start.2 = (f32[1024]{0:T(1024)S(1)}, f32[1024]{0:T(1024)}, u32[]{:S(2)}) copy-start(f32[1024]{0:T(1024)} %param.28) | copy-start | bytes 12292
Sparse Core Ops, SparseCore 0:
  13.8 43.1 all-gather.3
  59.1 76.5 all-gather.5
